TPU v7x, 256 devices: a whole 4x4x8 slice. The times are simulated.
256 devices in a mesh: fs: 32 (over z, x), tp: 8 (over y, core).
Axes of the slice: x: 4, y: 4, z: 8, core: 2. Of those that a mesh axis runs over, the one named last changes fastest.
Arguments:
- tokens: bfloat16 [32768, 2048], P(('fs', 'tp')), may hold values from -6 to 6
- gate_pre: bfloat16 [32768, 5632], P('fs', 'tp'), may hold values from -6 to 6
- value_pre: bfloat16 [32768, 5632], P('fs', 'tp'), may hold values from -6 to 6
- up_gate_w: bfloat16 [2048, 5632], P('fs', 'tp'), may hold values from -0.078125 to 0.078125
- up_value_w: bfloat16 [2048, 5632], P('fs', 'tp'), may hold values from -0.078125 to 0.078125
- conv_weight: float32 [3, 5632], P(None, 'tp'), may hold values from -3 to 3
- conv_bias: float32 [5632], P('tp'), may hold values from -3 to 3
- hidden_grad: bfloat16 [32768, 5632], P('fs', 'tp'), may hold values from -6 to 6
Outputs:
- input_grad: bfloat16 [32768, 2048], P(('fs', 'tp'))
- up_gate_grad: float32 [2048, 5632], P('fs', 'tp')
- up_value_grad: float32 [2048, 5632], P('fs', 'tp')
- conv_weight_grad: float32 [3, 5632], P(None, 'tp')
- conv_bias_grad: float32 [5632], P('tp')
All inputs are finite; a program needn't handle non-finite values.
Results may differ from a plain program's by a relative error of at most 0.013.
Values may be sent and summed in bfloat16 or wider, within the bound.
No kernel may reach another device: no remote copies, remote signals or barrier semaphores. Data moves between devices by JAX's collectives and lax.ppermute only.
A program may use at most 128 MiB of HBM per device.

v0:
```python
import jax
import jax.numpy as jnp
from jax import lax
from jax.sharding import Mesh
from jax.sharding import PartitionSpec as P

FS = ("fs_0", "fs_1")
FS_TP = ("fs_0", "fs_1", "tp")


def copy_for_each(shard, axis):
    peers = lax.axis_size(axis)
    return lax.all_to_all(
        jnp.broadcast_to(shard[None], (peers, *shard.shape)), axis, 0, 0, tiled=True
    )


def taken_together(shard, axis):
    return copy_for_each(shard, axis).sum(axis=0)


def in_one_piece(arrays, axis, dim, along):
    ends, at = ([], 0)
    for a in arrays[:-1]:
        at += a.shape[along]
        ends.append(at)
    both = jnp.concatenate(arrays, axis=along)
    return tuple(jnp.split(lax.all_gather(both, axis, axis=dim, tiled=True), ends, axis=along))


def summed_rows(subtotal, axes):
    return lax.psum_scatter(
        subtotal.astype(jnp.bfloat16), axes, scatter_dimension=0, tiled=True
    ).astype(jnp.float32)


def in_blocks(shard, dim, peers):
    lengths = shard.shape
    blocks = shard.reshape(*lengths[:dim], peers, lengths[dim] // peers, *lengths[dim + 1 :])
    return jnp.moveaxis(blocks, dim, 0)


def summed_on_arrival(shard, axis, dim):
    blocks = in_blocks(shard, dim, lax.axis_size(axis))
    arrived = lax.all_to_all(blocks, axis, split_axis=0, concat_axis=0, tiled=True)
    return arrived.astype(jnp.float32).sum(axis=0)


def contract_rows(left, right):
    return lax.dot_general(
        left, right, (((0,), (0,)), ((), ())), preferred_element_type=jnp.float32
    )


def contract_cols(left, right):
    return lax.dot_general(
        left, right, (((1,), (1,)), ((), ())), preferred_element_type=jnp.float32
    )


def on_device(
    tokens, gate_pre, value_pre, up_gate_w, up_value_w, conv_weight, conv_bias, hidden_grad
):
    length = gate_pre.shape[0]
    col_count = gate_pre.shape[1]
    scale = float(length * lax.axis_size(FS)) ** (-0.5)
    gate_float = gate_pre.astype(jnp.float32)
    padded = jnp.pad(gate_float, ((2, 0), (0, 0)))
    gate_conv = (
        conv_bias
        + conv_weight[0] * padded[:length]
        + conv_weight[1] * padded[1 : length + 1]
        + conv_weight[2] * padded[2:]
    )
    active, gelu_back = jax.vjp(jax.nn.gelu, gate_conv)
    grad_float = hidden_grad.astype(jnp.float32)
    value_grad = (grad_float * active).astype(jnp.bfloat16)
    conv_grad = gelu_back(grad_float * value_pre.astype(jnp.float32))[0]
    shifted = jnp.pad(conv_grad, ((0, 2), (0, 0)))
    gate_grad = (
        conv_weight[2] * conv_grad
        + conv_weight[1] * shifted[1 : length + 1]
        + conv_weight[0] * shifted[2:]
    ).astype(jnp.bfloat16)
    conv_terms = jnp.stack(
        [
            jnp.sum(conv_grad * padded[:length], axis=0),
            jnp.sum(conv_grad * padded[1 : length + 1], axis=0),
            jnp.sum(conv_grad * padded[2:], axis=0),
            jnp.sum(conv_grad, axis=0),
        ]
    )
    conv_total = taken_together(conv_terms, FS) * scale
    whole_tokens = lax.all_gather(tokens, "tp", axis=0, tiled=True)
    full_gate, full_value = in_one_piece((up_gate_w, up_value_w), FS, 0, 1)
    joined = summed_rows(
        jnp.concatenate(
            [contract_rows(whole_tokens, gate_grad), contract_rows(whole_tokens, value_grad)],
            axis=1,
        ),
        FS,
    )
    gate_out = joined[:, :col_count] * scale
    value_out = joined[:, col_count:] * scale
    input_grad = summed_on_arrival(
        (contract_cols(gate_grad, full_gate) + contract_cols(value_grad, full_value)).astype(
            jnp.bfloat16
        ),
        "tp",
        0,
    ).astype(jnp.bfloat16)
    return (input_grad, gate_out, value_out, conv_total[:3], conv_total[3])


def solution(mesh):
    finer = Mesh(mesh.devices.reshape(8, 4, mesh.shape["tp"]), ("fs_0", "fs_1", "tp"))
    in_specs = (
        P(FS_TP, None),
        P(FS, "tp"),
        P(FS, "tp"),
        P(FS, "tp"),
        P(FS, "tp"),
        P(None, "tp"),
        P("tp"),
        P(FS, "tp"),
    )
    out_specs = (P(FS_TP, None), P(FS, "tp"), P(FS, "tp"), P(None, "tp"), P("tp"))
    return jax.shard_map(
        on_device, mesh=finer, in_specs=in_specs, out_specs=out_specs, check_vma=False
    )
```

profile of v0, /device:TPU:8, one launch (start us, length us, event | category | flops | bytes accessed | tf_op | source)
XLA Modules:
  0.0 376.6 jit_solution(886776564580868433)
XLA Ops:
  7.3 0.7 all-gather.5.cloned.1.call-update
  8.0 1.8 pad_maximum_fusion.1
  9.9 1.8 convert_element_type.30
  11.8 6.5 %multiply_reduce_fusion.2 = (f32[704]{0:T(1024)S(1)}, f32[704]{0:T(1024)S(1)}, f32[704]{0:T(1024)S(1)}, f32[704]{0:T(1024)S(1)}, f32[1024,704]{0,1:T(8,128)S(1)}, /*index=5*/f32[1024,704]{0,1:T(8,128)}) fusion(f32[1024,704]{0,1:T(8,128)S(1)} %convert_element_type.30, bf16[1024,704]{0,1:T(8,128)(2,1)S(1)} %copy-done, bf16[1024,704]{0,1:T(8,128)(2,1)S(1)} %copy-done.2, ...), kind=kLoop, calls=%fused_computation.31 | loop fusion | flops 25949440 | bytes 12998656 | tf_op jit(solution)/shard_map/reduce_sum | solution.py:87
  18.3 3.0 fusion.8
  21.3 25.0 %all-gather.5.cloned.1.call-done = bf16[1024,2048]{1,0:T(8,128)(2,1)} async-done(((bf16[128,2048]{1,0:T(8,128)(2,1)}), bf16[1024,2048]{1,0:T(8,128)(2,1)}) %all-gather.5.cloned.1.call-update) | async-done | bytes 4194320 | tf_op jit(solution)/shard_map/all_gather | solution.py:94
  46.4 5.9 %fusion.3 = bf16[2048,704]{0,1:T(8,128)(2,1)S(1)} fusion(bf16[1024,704]{0,1:T(8,128)(2,1)} %fusion.8, bf16[1024,2048]{1,0:T(8,128)(2,1)} %all-gather.5.cloned.1.call-done), kind=kOutput, calls=%fused_computation.15 | convolution fusion | flops 2954231808 | bytes 8519680 | tf_op jit(solution)/shard_map/dot_general | solution.py:50
  52.3 3.9 %fusion.4 = bf16[2048,704]{0,1:T(8,128)(2,1)S(1)} fusion(bf16[1024,2048]{1,0:T(8,128)(2,1)S(1)} %copy-done.10, bf16[1024,704]{0,1:T(8,128)(2,1)S(1)} %copy-done.4, f32[1024,704]{0,1:T(8,128)S(1)} %copy-done.1), kind=kOutput, calls=%fused_computation.16 | convolution fusion | flops 2962161664 | bytes 11403264 | tf_op jit(solution)/shard_map/dot_general | solution.py:50
  56.2 3.1 pad_maximum_fusion
  59.4 8.4 %copy.22 = bf16[2048,1408]{1,0:T(8,128)(2,1)} copy(bf16[2048,1408]{0,1:T(8,128)(2,1)} %pad_maximum_fusion) | data formatting | bytes 11534336
  67.8 0.8 broadcast_in_dim.2
  68.6 10.0 %all-to-all-start.1 = ((f32[32,4,704]{2,1,0:T(4,128)}), f32[32,4,704]{2,1,0:T(4,128)S(1)}, u32[]{:S(2)}, u32[]{:S(2)}) async-start(f32[32,4,704]{2,1,0:T(4,128)} %broadcast_in_dim.2), calls=%async_computation.1 | async-start | bytes 786432 | tf_op jit(solution)/shard_map/all_to_all | solution.py:13
  78.7 60.2 %all-gather.3.cloned.1.call-done = bf16[2048,1408]{1,0:T(8,128)(2,1)} async-done(((bf16[64,1408]{1,0:T(8,128)(2,1)}), bf16[2048,1408]{1,0:T(8,128)(2,1)}) %all-gather.3.cloned.1.call-update) | async-done | bytes 5767184 | tf_op jit(solution)/shard_map/all_gather | solution.py:28
  138.9 6.0 %fusion.1 = f32[1024,2048]{1,0:T(8,128)S(1)} fusion(bf16[1024,704]{0,1:T(8,128)(2,1)} %fusion.8, bf16[2048,1408]{1,0:T(8,128)(2,1)} %all-gather.3.cloned.1.call-done), kind=kOutput, calls=%fused_computation.13 | convolution fusion | flops 2952790016 | bytes 12976128 | tf_op jit(solution)/shard_map/dot_general | solution.py:56
  144.9 7.6 %add_convert_fusion = bf16[1024,2048]{1,0:T(8,128)(2,1)} fusion(f32[1024,2048]{1,0:T(8,128)S(1)} %fusion.1, bf16[2048,1408]{1,0:T(8,128)(2,1)S(1)} %copy-done.9, bf16[1024,704]{0,1:T(8,128)(2,1)S(1)} %copy-done.5, f32[1024,704]{0,1:T(8,128)S(1)} %copy-done.1), kind=kOutput, calls=%fused_computation | convolution fusion | flops 2964914176 | bytes 20054016 | tf_op jit(solution)/shard_map/dot_general | solution.py:56
  152.5 5.0 %all-to-all-start = ((bf16[8,128,2048]{2,1,0:T(8,128)(2,1)}), bf16[8,128,2048]{2,1,0:T(8,128)(2,1)}, u32[]{:S(2)}, u32[]{:S(2)}) async-start(bf16[8,128,2048]{2,1,0:T(8,128)(2,1)} %bitcast.11), calls=%async_computation | async-start | bytes 8388608 | tf_op jit(solution)/shard_map/all_to_all | solution.py:45
  157.4 0.1 reduce_sum.62
  157.5 0.6 slice_reduce_fusion
  158.1 47.6 %all-to-all-done = bf16[8,128,2048]{2,1,0:T(8,128)(2,1)} async-done(((bf16[8,128,2048]{2,1,0:T(8,128)(2,1)}), bf16[8,128,2048]{2,1,0:T(8,128)(2,1)}, u32[]{:S(2)}, u32[]{:S(2)}) %all-to-all-start) | async-done | bytes 4194336 | tf_op jit(solution)/shard_map/all_to_all | solution.py:45
  205.8 4.0 %reduce_sum.57 = bf16[128,2048]{1,0:T(8,128)(2,1)} reduce(bf16[8,128,2048]{2,1,0:T(8,128)(2,1)} %all-to-all-done, bf16[]{:T(256)} %constant.19.clone.1), dimensions={0}, to_apply=%region_0.1 | reduce | flops 1835008 | bytes 4718594 | tf_op jit(solution)/shard_map/reduce_sum | solution.py:46
  209.7 157.4 %reduce-scatter.4.cloned.1.call-done = bf16[64,1408]{1,0:T(8,128)(2,1)} async-done(((bf16[2048,1408]{1,0:T(8,128)(2,1)}), bf16[64,1408]{1,0:T(8,128)(2,1)}) %reduce-scatter.4.cloned.1.call-update) | async-done | bytes 180240
  367.2 1.1 copy.23
  368.4 0.8 copy.21
  369.3 0.8 copy.20
  (37 shorter events, 0.4 us)
Async XLA Ops:
  7.2 4.6 %copy-start = (bf16[1024,704]{0,1:T(8,128)(2,1)S(1)}, bf16[1024,704]{0,1:T(8,128)(2,1)}, u32[]{:S(2)}) copy-start(bf16[1024,704]{0,1:T(8,128)(2,1)} %param.9) | copy-start | bytes 4325380
  7.2 4.5 %copy-start.7 = (f32[3,704]{1,0:T(4,128)S(1)}, f32[3,704]{1,0:T(4,128)}, u32[]{:S(2)}) copy-start(f32[3,704]{1,0:T(4,128)} %param.13) | copy-start | bytes 25348
  7.2 4.6 %copy-start.8 = (f32[704]{0:T(1024)S(1)}, f32[704]{0:T(1024)}, u32[]{:S(2)}) copy-start(f32[704]{0:T(1024)} %param.14) | copy-start | bytes 8452
  7.2 4.6 %copy-start.2 = (bf16[1024,704]{0,1:T(8,128)(2,1)S(1)}, bf16[1024,704]{0,1:T(8,128)(2,1)}, u32[]{:S(2)}) copy-start(bf16[1024,704]{0,1:T(8,128)(2,1)} %param.10) | copy-start | bytes 4325380
  7.2 39.2 %all-gather.5.cloned.1.call-start = ((), (), s32[]{:S(2)}) async-start(), calls=%async_computation.4 | async-start | bytes 4718592 | tf_op jit(solution)/shard_map/all_gather | solution.py:94
  7.9 131.0 %all-gather.3.cloned.1.call-start = ((), (), s32[]{:S(2)}) async-start(), calls=%async_computation.3 | async-start | bytes 5947392 | tf_op jit(solution)/shard_map/all_gather | solution.py:28
  9.8 357.4 %reduce-scatter.4.cloned.1.call-start = ((), (), s32[]{:S(2)}) async-start(), calls=%async_computation.5 | async-start | bytes 5947392
  9.9 1.9 copy-start.3
  21.3 31.0 %copy-start.1 = (f32[1024,704]{0,1:T(8,128)S(1)}, f32[1024,704]{0,1:T(8,128)}, u32[]{:S(2)}) copy-start(f32[1024,704]{0,1:T(8,128)} %get-tuple-element.33) | copy-start | bytes 8650756
  46.4 5.9 %copy-start.4 = (bf16[1024,704]{0,1:T(8,128)(2,1)S(1)}, bf16[1024,704]{0,1:T(8,128)(2,1)}, u32[]{:S(2)}) copy-start(bf16[1024,704]{0,1:T(8,128)(2,1)} %param.15) | copy-start | bytes 4325380
  46.4 5.9 %copy-start.10 = (bf16[1024,2048]{1,0:T(8,128)(2,1)S(1)}, bf16[1024,2048]{1,0:T(8,128)(2,1)}, u32[]{:S(2)}) copy-start(bf16[1024,2048]{1,0:T(8,128)(2,1)} %all-gather.5.cloned.1.call-done) | copy-start | bytes 12582916
  68.6 83.8 %all-to-all-start.1 = ((f32[32,4,704]{2,1,0:T(4,128)}), f32[32,4,704]{2,1,0:T(4,128)S(1)}, u32[]{:S(2)}, u32[]{:S(2)}) async-start(f32[32,4,704]{2,1,0:T(4,128)} %broadcast_in_dim.2), calls=%async_computation.1 | async-start | bytes 786432 | tf_op jit(solution)/shard_map/all_to_all | solution.py:13
  138.9 6.0 %copy-start.5 = (bf16[1024,704]{0,1:T(8,128)(2,1)S(1)}, bf16[1024,704]{0,1:T(8,128)(2,1)}, u32[]{:S(2)}) copy-start(bf16[1024,704]{0,1:T(8,128)(2,1)} %param.15) | copy-start | bytes 4325380
  138.9 6.0 %copy-start.9 = (bf16[2048,1408]{1,0:T(8,128)(2,1)S(1)}, bf16[2048,1408]{1,0:T(8,128)(2,1)}, u32[]{:S(2)}) copy-start(bf16[2048,1408]{1,0:T(8,128)(2,1)} %all-gather.3.cloned.1.call-done) | copy-start | bytes 17301508
  152.5 53.3 %all-to-all-start = ((bf16[8,128,2048]{2,1,0:T(8,128)(2,1)}), bf16[8,128,2048]{2,1,0:T(8,128)(2,1)}, u32[]{:S(2)}, u32[]{:S(2)}) async-start(bf16[8,128,2048]{2,1,0:T(8,128)(2,1)} %bitcast.11), calls=%async_computation | async-start | bytes 8388608 | tf_op jit(solution)/shard_map/all_to_all | solution.py:45
  157.5 210.8 %copy-start.6 = (f32[4,704]{1,0:T(4,128)}, f32[4,704]{1,0:T(4,128)S(1)}, u32[]{:S(2)}) copy-start(f32[4,704]{1,0:T(4,128)S(1)} %broadcast_multiply_fusion) | copy-start | bytes 33796
Sparse Core Ops, SparseCore 0:
  9.9 36.4 all-gather.4
  49.5 89.3 all-gather.2
  142.9 224.2 reduce-scatter.3
where the time goes:
time: 377 us
  waiting for transfers between devices  291 us (77%)
  matrix products  23.3 us (6%)
  other arithmetic  20.5 us (5%)
  starting transfers between devices  15.1 us (4%)
  between operations  14 us (4%)
  local copies, waits for them, and re-layouts  12.7 us (3%)
    unnamed x4, waiting for transfers between devices  158 us
    all_gather x1, waiting for transfers between devices, in_one_piece(): lax.all_gather(both, axis, axis=dim, tiled=True)  60.2 us
    all_to_all x1, waiting for transfers between devices, summed_on_arrival(): lax.all_to_all(blocks, axis, split_axis=0, concat_axis=0, tiled=True)  47.6 us
    all_gather x1, waiting for transfers between devices, on_device(): whole_tokens = lax.all_gather(tokens, 'tp', axis=0, tiled=True)  25 us
    dot_general x2, matrix products, contract_cols(): lax.dot_general(left, right, (((1,), (1,)), ((), ())), preferred_element_...  13.5 us
    unnamed x26, local copies, waits for them, and re-layouts  11.2 us
    all_to_all x1, starting transfers between devices, copy_for_each(): lax.all_to_all(jnp.broadcast_to(shard[None], (peers, *shard.shape)), axis...  10 us
    dot_general x2, matrix products, contract_rows(): lax.dot_general(left, right, (((0,), (0,)), ((), ())), preferred_element_...  9.78 us
  transfers between devices with their start and end apart: 5, of which 4 were waited for; matrix products, arithmetic and copies ran while one was open for 14% of the time, Pallas kernels for 0%

commit v1 on v0

--- a/solution.py
+++ b/solution.py
@@ -91,7 +91,12 @@
         ]
     )
     conv_total = taken_together(conv_terms, FS) * scale
-    whole_tokens = lax.all_gather(tokens, "tp", axis=0, tiled=True)
+    ring = [tokens]
+    for hop in range(7):
+        ring.append(lax.ppermute(ring[-1], "tp", [(dev, (dev + 1) % 8) for dev in range(8)]))
+    whole_tokens = jnp.roll(
+        jnp.concatenate(ring[::-1], axis=0), (lax.axis_index("tp") + 1) * ring[0].shape[0], axis=0
+    )
     full_gate, full_value = in_one_piece((up_gate_w, up_value_w), FS, 0, 1)
     joined = summed_rows(
         jnp.concatenate(

time: 377 us -> 343 us (0.910)
  waiting for transfers between devices: 291 us -> 246 us
  starting transfers between devices: 15.1 us -> 23.2 us
  local copies, waits for them, and re-layouts: 12.7 us -> 18.3 us
    all_gather x1, waiting for transfers between devices: 60.2 us -> 0.02 us  [in_one_piece(): lax.all_gather(both, axis, axis=dim, tiled=True)]
    ppermute x0 -> x7, waiting for transfers between devices: none -> 50.1 us  [on_device(): lax.ppermute(ring[-1], 'tp', [(dev, (dev + 1) % 8) for dev in range(8)])]
    all_gather x1 -> x0, waiting for transfers between devices: 25 us -> none  [on_device(): whole_tokens = lax.all_gather(tokens, 'tp', axis=0, tiled=True)]
    unnamed x4 -> x3, waiting for transfers between devices: 158 us -> 146 us
    all_to_all x1, starting transfers between devices: 4.97 us -> 11.6 us  [summed_on_arrival(): lax.all_to_all(blocks, axis, split_axis=0, concat_axis=0, tiled=True)]
    unnamed x26 -> x59, local copies, waits for them, and re-layouts: 11.2 us -> 16.8 us
  transfers between devices with their start and end apart: 5 -> 11, of which waited for: 4 -> 10; matrix products, arithmetic and copies ran while one was open for 14% -> 16% of each run, Pallas kernels for 0% -> 0%
where the time goes in v1:
time: 343 us
  waiting for transfers between devices  246 us (72%)
  starting transfers between devices  23.2 us (7%)
  matrix products  21.3 us (6%)
  other arithmetic  19.5 us (6%)
  local copies, waits for them, and re-layouts  18.3 us (5%)
  between operations  14.5 us (4%)
    unnamed x3, waiting for transfers between devices  146 us
    ppermute x7, waiting for transfers between devices, on_device(): lax.ppermute(ring[-1], 'tp', [(dev, (dev + 1) % 8) for dev in range(8)])  50.1 us
    all_to_all x1, waiting for transfers between devices, summed_on_arrival(): lax.all_to_all(blocks, axis, split_axis=0, concat_axis=0, tiled=True)  47.6 us
    unnamed x59, local copies, waits for them, and re-layouts  16.8 us
    dot_general x2, matrix products, contract_cols(): lax.dot_general(left, right, (((1,), (1,)), ((), ())), preferred_element_...  13.6 us
    all_to_all x1, starting transfers between devices, summed_on_arrival(): lax.all_to_all(blocks, axis, split_axis=0, concat_axis=0, tiled=True)  11.6 us
    all_to_all x1, starting transfers between devices, copy_for_each(): lax.all_to_all(jnp.broadcast_to(shard[None], (peers, *shard.shape)), axis...  11.5 us
    dot_general x2, matrix products, contract_rows(): lax.dot_general(left, right, (((0,), (0,)), ((), ())), preferred_element_...  7.73 us
  transfers between devices with their start and end apart: 11, of which 10 were waited for; matrix products, arithmetic and copies ran while one was open for 16% of the time, Pallas kernels for 0%

profile of v1, /device:TPU:8, one launch (start us, length us, event | category | flops | bytes accessed | tf_op | source)
XLA Modules:
  0.0 342.7 jit_solution(10365677605329927463)
XLA Ops:
  7.2 1.7 pad_maximum_fusion.1
  9.1 8.8 %collective-permute-done = bf16[128,2048]{1,0:T(8,128)(2,1)S(1)} collective-permute-done((bf16[128,2048]{1,0:T(8,128)(2,1)}, bf16[128,2048]{1,0:T(8,128)(2,1)S(1)}, u32[]{:S(2)}, u32[]{:S(2)}) %collective-permute-start) | collective-permute-done | bytes 524320 | tf_op jit(solution)/shard_map/ppermute | solution.py:96
  17.9 8.6 %collective-permute-done.1 = bf16[128,2048]{1,0:T(8,128)(2,1)S(1)} collective-permute-done((bf16[128,2048]{1,0:T(8,128)(2,1)S(1)}, bf16[128,2048]{1,0:T(8,128)(2,1)S(1)}, u32[]{:S(2)}, u32[]{:S(2)}) %collective-permute-start.1) | collective-permute-done | bytes 524320 | tf_op jit(solution)/shard_map/ppermute | solution.py:96
  26.5 8.6 %collective-permute-done.2 = bf16[128,2048]{1,0:T(8,128)(2,1)S(1)} collective-permute-done((bf16[128,2048]{1,0:T(8,128)(2,1)S(1)}, bf16[128,2048]{1,0:T(8,128)(2,1)S(1)}, u32[]{:S(2)}, u32[]{:S(2)}) %collective-permute-start.2) | collective-permute-done | bytes 524320 | tf_op jit(solution)/shard_map/ppermute | solution.py:96
  35.1 8.6 %collective-permute-done.3 = bf16[128,2048]{1,0:T(8,128)(2,1)S(1)} collective-permute-done((bf16[128,2048]{1,0:T(8,128)(2,1)S(1)}, bf16[128,2048]{1,0:T(8,128)(2,1)S(1)}, u32[]{:S(2)}, u32[]{:S(2)}) %collective-permute-start.3) | collective-permute-done | bytes 524320 | tf_op jit(solution)/shard_map/ppermute | solution.py:96
  43.7 8.6 %collective-permute-done.4 = bf16[128,2048]{1,0:T(8,128)(2,1)S(1)} collective-permute-done((bf16[128,2048]{1,0:T(8,128)(2,1)S(1)}, bf16[128,2048]{1,0:T(8,128)(2,1)S(1)}, u32[]{:S(2)}, u32[]{:S(2)}) %collective-permute-start.4) | collective-permute-done | bytes 524320 | tf_op jit(solution)/shard_map/ppermute | solution.py:96
  52.4 1.9 convert_element_type.30
  54.3 6.7 %collective-permute-done.5 = bf16[128,2048]{1,0:T(8,128)(2,1)} collective-permute-done((bf16[128,2048]{1,0:T(8,128)(2,1)S(1)}, bf16[128,2048]{1,0:T(8,128)(2,1)}, u32[]{:S(2)}, u32[]{:S(2)}) %collective-permute-start.5) | collective-permute-done | bytes 524320 | tf_op jit(solution)/shard_map/ppermute | solution.py:96
  61.1 6.6 %multiply_reduce_fusion.2 = (f32[704]{0:T(1024)S(1)}, f32[704]{0:T(1024)S(1)}, f32[704]{0:T(1024)S(1)}, f32[704]{0:T(1024)S(1)}, f32[1024,704]{0,1:T(8,128)S(1)}, /*index=5*/f32[1024,704]{0,1:T(8,128)}) fusion(f32[1024,704]{0,1:T(8,128)S(1)} %convert_element_type.30, bf16[1024,704]{0,1:T(8,128)(2,1)S(1)} %copy-done, bf16[1024,704]{0,1:T(8,128)(2,1)S(1)} %copy-done.11, ...), kind=kLoop, calls=%fused_computation.33 | loop fusion | flops 25949440 | bytes 12998656 | tf_op jit(solution)/shard_map/reduce_sum | solution.py:87
  67.7 2.1 fusion.16
  70.0 1.7 constant_dynamic-update-slice_fusion.15
  71.7 1.2 constant_dynamic-update-slice_fusion.14
  75.7 3.4 fusion.7
  79.1 4.3 %fusion.4 = bf16[2048,704]{0,1:T(8,128)(2,1)S(1)} fusion(bf16[2048,2048]{1,0:T(8,128)(2,1)S(1)} %constant_dynamic-update-slice_fusion, s32[]{:T(128)S(6)} %select_n.14, bf16[1024,704]{0,1:T(8,128)(2,1)S(1)} %copy-done.13, f32[1024,704]{0,1:T(8,128)S(1)} %copy-done.1), kind=kOutput, calls=%fused_computation.10 | convolution fusion | flops 2962161664 | bytes 11403268 | tf_op jit(solution)/shard_map/dot_general | solution.py:50
  83.4 3.2 pad_maximum_fusion
  86.6 8.4 %copy.22 = bf16[2048,1408]{1,0:T(8,128)(2,1)} copy(bf16[2048,1408]{0,1:T(8,128)(2,1)} %pad_maximum_fusion) | data formatting | bytes 11534336
  95.9 11.5 %all-to-all-start.1 = ((f32[32,4,704]{2,1,0:T(4,128)}), f32[32,4,704]{2,1,0:T(4,128)S(1)}, u32[]{:S(2)}, u32[]{:S(2)}) async-start(f32[32,4,704]{2,1,0:T(4,128)} %broadcast_in_dim.2), calls=%async_computation.1 | async-start | bytes 786432 | tf_op jit(solution)/shard_map/all_to_all | solution.py:13
  107.5 6.0 %fusion.11 = f32[1024,2048]{1,0:T(8,128)S(1)} fusion(bf16[1024,704]{0,1:T(8,128)(2,1)} %copy-done.15, bf16[2048,1408]{1,0:T(8,128)(2,1)} %all-gather.2.cloned.1.call-done), kind=kOutput, calls=%fused_computation.17 | convolution fusion | flops 2952790016 | bytes 12976128 | tf_op jit(solution)/shard_map/dot_general | solution.py:56
  113.5 7.6 %add_convert_fusion = bf16[1024,2048]{1,0:T(8,128)(2,1)} fusion(f32[1024,2048]{1,0:T(8,128)S(1)} %fusion.11, bf16[2048,1408]{1,0:T(8,128)(2,1)S(1)} %copy-done.19, bf16[1024,704]{0,1:T(8,128)(2,1)S(1)} %copy-done.14, f32[1024,704]{0,1:T(8,128)S(1)} %copy-done.1), kind=kOutput, calls=%fused_computation | convolution fusion | flops 2964914176 | bytes 20054016 | tf_op jit(solution)/shard_map/dot_general | solution.py:56
  121.0 2.2 all-to-all-done.1
  123.3 11.6 %all-to-all-start = ((bf16[8,128,2048]{2,1,0:T(8,128)(2,1)}), bf16[8,128,2048]{2,1,0:T(8,128)(2,1)}, u32[]{:S(2)}, u32[]{:S(2)}) async-start(bf16[8,128,2048]{2,1,0:T(8,128)(2,1)} %bitcast.5), calls=%async_computation | async-start | bytes 8388608 | tf_op jit(solution)/shard_map/all_to_all | solution.py:45
  135.6 47.6 %all-to-all-done = bf16[8,128,2048]{2,1,0:T(8,128)(2,1)} async-done(((bf16[8,128,2048]{2,1,0:T(8,128)(2,1)}), bf16[8,128,2048]{2,1,0:T(8,128)(2,1)}, u32[]{:S(2)}, u32[]{:S(2)}) %all-to-all-start) | async-done | bytes 4194336 | tf_op jit(solution)/shard_map/all_to_all | solution.py:45
  183.2 3.9 %reduce_sum.57 = bf16[128,2048]{1,0:T(8,128)(2,1)} reduce(bf16[8,128,2048]{2,1,0:T(8,128)(2,1)} %all-to-all-done, bf16[]{:T(256)} %constant.42.clone.1), dimensions={0}, to_apply=%region_0.1 | reduce | flops 1835008 | bytes 4718594 | tf_op jit(solution)/shard_map/reduce_sum | solution.py:46
  187.1 145.9 %reduce-scatter.4.cloned.1.call-done = bf16[64,1408]{1,0:T(8,128)(2,1)} async-done(((bf16[2048,1408]{1,0:T(8,128)(2,1)}), bf16[64,1408]{1,0:T(8,128)(2,1)}) %reduce-scatter.4.cloned.1.call-update) | async-done | bytes 180240
  (82 shorter events, 7.5 us)
Async XLA Ops:
  7.2 47.1 %copy-start.17 = (f32[3,704]{1,0:T(4,128)S(1)}, f32[3,704]{1,0:T(4,128)}, u32[]{:S(2)}) copy-start(f32[3,704]{1,0:T(4,128)} %param.13) | copy-start | bytes 25348
  7.2 53.9 %copy-start.18 = (f32[704]{0:T(1024)S(1)}, f32[704]{0:T(1024)}, u32[]{:S(2)}) copy-start(f32[704]{0:T(1024)} %param.14) | copy-start | bytes 8452
  7.2 100.3 %all-gather.2.cloned.1.call-start = ((), (), s32[]{:S(2)}) async-start(), calls=%async_computation.3 | async-start | bytes 5947392 | tf_op jit(solution)/shard_map/all_gather | solution.py:28
  9.0 324.0 %reduce-scatter.4.cloned.1.call-start = ((), (), s32[]{:S(2)}) async-start(), calls=%async_computation.4 | async-start | bytes 5947392
  9.0 52.1 %copy-start = (bf16[1024,704]{0,1:T(8,128)(2,1)S(1)}, bf16[1024,704]{0,1:T(8,128)(2,1)}, u32[]{:S(2)}) copy-start(bf16[1024,704]{0,1:T(8,128)(2,1)} %param.9) | copy-start | bytes 4325380
  9.0 52.1 %copy-start.11 = (bf16[1024,704]{0,1:T(8,128)(2,1)S(1)}, bf16[1024,704]{0,1:T(8,128)(2,1)}, u32[]{:S(2)}) copy-start(bf16[1024,704]{0,1:T(8,128)(2,1)} %param.10) | copy-start | bytes 4325380
  9.0 52.1 %copy-start.12 = (bf16[1024,704]{0,1:T(8,128)(2,1)S(1)}, bf16[1024,704]{0,1:T(8,128)(2,1)}, u32[]{:S(2)}) copy-start(bf16[1024,704]{0,1:T(8,128)(2,1)} %param.15) | copy-start | bytes 4325380
  9.1 8.8 %collective-permute-start = (bf16[128,2048]{1,0:T(8,128)(2,1)}, bf16[128,2048]{1,0:T(8,128)(2,1)S(1)}, u32[]{:S(2)}, u32[]{:S(2)}) collective-permute-start(bf16[128,2048]{1,0:T(8,128)(2,1)} %param.8), channel_id=1, source_target_pairs={{0,1},{1,2},{2,3},{3,4},{4,5},{5,6},{6,7},{7,0},{8,9},{9,10},{10,1... | collective-permute-start | bytes 1572872 | tf_op jit(solution)/shard_map/ppermute | solution.py:96
  17.9 8.6 %collective-permute-start.1 = (bf16[128,2048]{1,0:T(8,128)(2,1)S(1)}, bf16[128,2048]{1,0:T(8,128)(2,1)S(1)}, u32[]{:S(2)}, u32[]{:S(2)}) collective-permute-start(bf16[128,2048]{1,0:T(8,128)(2,1)S(1)} %collective-permute-done), channel_id=1, source_target_pairs={{0,1},{1,2},{2,3},{3,4},{4,5},{5,6},{6,7},{7,0},{8,9},{9,10},{10,1... | collective-permute-start | bytes 1572872 | tf_op jit(solution)/shard_map/ppermute | solution.py:96
  26.5 25.8 %copy-start.3 = (bf16[128,2048]{1,0:T(8,128)(2,1)}, bf16[128,2048]{1,0:T(8,128)(2,1)S(1)}, u32[]{:S(2)}) copy-start(bf16[128,2048]{1,0:T(8,128)(2,1)S(1)} %collective-permute-done.1) | copy-start | bytes 1572868
  26.5 8.6 %collective-permute-start.2 = (bf16[128,2048]{1,0:T(8,128)(2,1)S(1)}, bf16[128,2048]{1,0:T(8,128)(2,1)S(1)}, u32[]{:S(2)}, u32[]{:S(2)}) collective-permute-start(bf16[128,2048]{1,0:T(8,128)(2,1)S(1)} %collective-permute-done.1), channel_id=1, source_target_pairs={{0,1},{1,2},{2,3},{3,4},{4,5},{5,6},{6,7},{7,0},{8,9},{9,10},{10,1... | collective-permute-start | bytes 1572872 | tf_op jit(solution)/shard_map/ppermute | solution.py:96
  35.1 17.2 %copy-start.5 = (bf16[128,2048]{1,0:T(8,128)(2,1)}, bf16[128,2048]{1,0:T(8,128)(2,1)S(1)}, u32[]{:S(2)}) copy-start(bf16[128,2048]{1,0:T(8,128)(2,1)S(1)} %collective-permute-done.2) | copy-start | bytes 1572868
  35.1 8.6 %collective-permute-start.3 = (bf16[128,2048]{1,0:T(8,128)(2,1)S(1)}, bf16[128,2048]{1,0:T(8,128)(2,1)S(1)}, u32[]{:S(2)}, u32[]{:S(2)}) collective-permute-start(bf16[128,2048]{1,0:T(8,128)(2,1)S(1)} %collective-permute-done.2), channel_id=1, source_target_pairs={{0,1},{1,2},{2,3},{3,4},{4,5},{5,6},{6,7},{7,0},{8,9},{9,10},{10,1... | collective-permute-start | bytes 1572872 | tf_op jit(solution)/shard_map/ppermute | solution.py:96
  43.7 8.6 %copy-start.7 = (bf16[128,2048]{1,0:T(8,128)(2,1)}, bf16[128,2048]{1,0:T(8,128)(2,1)S(1)}, u32[]{:S(2)}) copy-start(bf16[128,2048]{1,0:T(8,128)(2,1)S(1)} %collective-permute-done.3) | copy-start | bytes 1572868
  43.7 8.6 %collective-permute-start.4 = (bf16[128,2048]{1,0:T(8,128)(2,1)S(1)}, bf16[128,2048]{1,0:T(8,128)(2,1)S(1)}, u32[]{:S(2)}, u32[]{:S(2)}) collective-permute-start(bf16[128,2048]{1,0:T(8,128)(2,1)S(1)} %collective-permute-done.3), channel_id=1, source_target_pairs={{0,1},{1,2},{2,3},{3,4},{4,5},{5,6},{6,7},{7,0},{8,9},{9,10},{10,1... | collective-permute-start | bytes 1572872 | tf_op jit(solution)/shard_map/ppermute | solution.py:96
  52.3 8.7 %copy-start.9 = (bf16[128,2048]{1,0:T(8,128)(2,1)}, bf16[128,2048]{1,0:T(8,128)(2,1)S(1)}, u32[]{:S(2)}) copy-start(bf16[128,2048]{1,0:T(8,128)(2,1)S(1)} %collective-permute-done.4) | copy-start | bytes 1572868
  52.3 8.7 %collective-permute-start.5 = (bf16[128,2048]{1,0:T(8,128)(2,1)S(1)}, bf16[128,2048]{1,0:T(8,128)(2,1)}, u32[]{:S(2)}, u32[]{:S(2)}) collective-permute-start(bf16[128,2048]{1,0:T(8,128)(2,1)S(1)} %collective-permute-done.4), channel_id=1, source_target_pairs={{0,1},{1,2},{2,3},{3,4},{4,5},{5,6},{6,7},{7,0},{8,9},{9,10},{10,1... | collective-permute-start | bytes 1572872 | tf_op jit(solution)/shard_map/ppermute | solution.py:96
  61.1 8.9 %collective-permute-start.6 = (bf16[128,2048]{1,0:T(8,128)(2,1)}, bf16[128,2048]{1,0:T(8,128)(2,1)}, u32[]{:S(2)}, u32[]{:S(2)}) collective-permute-start(bf16[128,2048]{1,0:T(8,128)(2,1)} %collective-permute-done.5), channel_id=1, source_target_pairs={{0,1},{1,2},{2,3},{3,4},{4,5},{5,6},{6,7},{7,0},{8,9},{9,10},{10,1... | collective-permute-start | bytes 1572872 | tf_op jit(solution)/shard_map/ppermute | solution.py:96
  69.8 5.8 %copy-start.15 = (bf16[1024,704]{0,1:T(8,128)(2,1)}, bf16[1024,704]{0,1:T(8,128)(2,1)S(1)}, u32[]{:S(2)}) copy-start(bf16[1024,704]{0,1:T(8,128)(2,1)S(1)} %fusion.16) | copy-start | bytes 4325380
  95.9 27.3 %all-to-all-start.1 = ((f32[32,4,704]{2,1,0:T(4,128)}), f32[32,4,704]{2,1,0:T(4,128)S(1)}, u32[]{:S(2)}, u32[]{:S(2)}) async-start(f32[32,4,704]{2,1,0:T(4,128)} %broadcast_in_dim.2), calls=%async_computation.1 | async-start | bytes 786432 | tf_op jit(solution)/shard_map/all_to_all | solution.py:13
  107.5 6.0 %copy-start.14 = (bf16[1024,704]{0,1:T(8,128)(2,1)S(1)}, bf16[1024,704]{0,1:T(8,128)(2,1)}, u32[]{:S(2)}) copy-start(bf16[1024,704]{0,1:T(8,128)(2,1)} %param.15) | copy-start | bytes 4325380
  107.5 6.0 %copy-start.19 = (bf16[2048,1408]{1,0:T(8,128)(2,1)S(1)}, bf16[2048,1408]{1,0:T(8,128)(2,1)}, u32[]{:S(2)}) copy-start(bf16[2048,1408]{1,0:T(8,128)(2,1)} %all-gather.2.cloned.1.call-done) | copy-start | bytes 17301508
  123.3 59.9 %all-to-all-start = ((bf16[8,128,2048]{2,1,0:T(8,128)(2,1)}), bf16[8,128,2048]{2,1,0:T(8,128)(2,1)}, u32[]{:S(2)}, u32[]{:S(2)}) async-start(bf16[8,128,2048]{2,1,0:T(8,128)(2,1)} %bitcast.5), calls=%async_computation | async-start | bytes 8388608 | tf_op jit(solution)/shard_map/all_to_all | solution.py:45
  135.0 199.2 %copy-start.16 = (f32[4,704]{1,0:T(4,128)}, f32[4,704]{1,0:T(4,128)S(1)}, u32[]{:S(2)}) copy-start(f32[4,704]{1,0:T(4,128)S(1)} %broadcast_multiply_fusion) | copy-start | bytes 33796
  (7 other events, 25.1 us)
Sparse Core Ops, SparseCore 0:
  11.1 89.4 all-gather.1
  104.6 228.3 reduce-scatter.3
